TPU v7x, 32 devices: a whole 2x2x4 slice. The times are simulated.
32 devices in a mesh: sp: 4 (over z), fs: 4 (over y, x), tp: 2 (over core).
Axes of the slice: x: 2, y: 2, z: 4, core: 2. Of those that a mesh axis runs over, the one named last changes fastest.
Arguments:
- tokens: bfloat16 [4, 2048, 2048], P('fs', ('sp', 'tp')), may hold values from -6 to 6
- norm_gain: float32 [2048], replicated, may hold values from 0.1 to 1.9
- query_weight: bfloat16 [2048, 1024], P('sp', 'tp'), may hold values from -20 to 20
- key_matrix: bfloat16 [2048, 256], P('sp', 'tp'), may hold values from -0.125 to 0.125
- value_matrix: bfloat16 [2048, 256], P('sp', 'tp'), may hold values from -0.125 to 0.125
- pool_in_weight: bfloat16 [2048, 1024], P('sp', 'tp'), may hold values from -0.125 to 0.125
- head_sink_logit: float32 [16], replicated, may hold values from 2 to 6
- pool_mix: bfloat16 [4, 256, 256], replicated, may hold values from -0.375 to 0.375
- pool_gain: float32 [1024], replicated, may hold values from 0.1 to 1.9
- attn_out_weight: bfloat16 [1024, 2048], P('tp', 'sp'), may hold values from -1 to 1
- pool_out_weight: bfloat16 [1024, 2048], P('tp', 'sp'), may hold values from -0.125 to 0.125
Outputs:
- mixed: bfloat16 [4, 2048, 2048], P('fs', ('sp', 'tp'))
- row_log_weight_sum: float32 [4, 16, 2048], P('fs', 'tp', 'sp')
All inputs are finite; a program needn't handle non-finite values.
Results may differ from a plain program's by a relative error of at most 0.0095.
The roundings to bfloat16 on the way count: a program that leaves them out, or rounds other values in their place, can miss the bound.
Values may be sent and summed in bfloat16 or wider, within the bound.
No kernel may reach another device: no remote copies, remote signals or barrier semaphores. Data moves between devices by JAX's collectives and lax.ppermute only.
A program may use at most 64 MiB of HBM per device.

v0:
```python
import jax
import jax.numpy as jnp
from jax import lax
from jax.sharding import PartitionSpec as P

HEAD_SIZE = 64
WINDOW = 128
POOL_CH = 256
EPSILON = 1e-06
POOL_SPANS = (2, 4, 8, 16)


def passed_along(shard, axis, by):
    size = lax.axis_size(axis)
    pairs = [(i, i + by) for i in range(size) if 0 <= i + by < size]
    return lax.ppermute(shard, axis, pairs)


def windowed_attend(
    query_rows, key_rows, value_rows, key_tail, value_tail, sinks, kv_heads, group, first_pos
):
    rows = query_rows.shape[0]
    blocks = rows // WINDOW
    width = key_rows.shape[1]
    ext_keys = jnp.concatenate([key_tail, key_rows], 0)
    ext_values = jnp.concatenate([value_tail, value_rows], 0)

    def banded(table):
        return jnp.concatenate(
            [
                table[:rows].reshape(blocks, WINDOW, width),
                table[WINDOW:].reshape(blocks, WINDOW, width),
            ],
            axis=1,
        )

    band_keys = banded(ext_keys).reshape(blocks, 2 * WINDOW, kv_heads, HEAD_SIZE)
    band_values = banded(ext_values).reshape(blocks, 2 * WINDOW, kv_heads, HEAD_SIZE)
    query_blocks = query_rows.reshape(blocks, WINDOW, kv_heads, group, HEAD_SIZE)
    scores = jnp.einsum(
        "bqkgd,bskd->bkgqs", query_blocks, band_keys, preferred_element_type=jnp.float32
    ) * HEAD_SIZE ** (-0.5)
    query_pos = first_pos + jnp.arange(rows).reshape(blocks, WINDOW, 1)
    key_pos = (
        first_pos
        - WINDOW
        + jnp.arange(blocks).reshape(blocks, 1, 1) * WINDOW
        + jnp.arange(2 * WINDOW).reshape(1, 1, 2 * WINDOW)
    )
    offset = query_pos - key_pos
    allowed = (offset >= 0) & (offset < WINDOW) & (key_pos >= 0)
    scores = jnp.where(allowed[:, None, None], scores, -jnp.inf)
    sink_grid = sinks.reshape(1, kv_heads, group, 1, 1)
    top = jnp.maximum(jnp.max(scores, axis=-1, keepdims=True), sink_grid)
    weights = jnp.exp(scores - top)
    total = jnp.sum(weights, axis=-1, keepdims=True) + jnp.exp(sink_grid - top)
    probs = (weights / total).astype(jnp.bfloat16)
    mixed = jnp.einsum(
        "bkgqs,bskd->bqkgd", probs, band_values, preferred_element_type=jnp.float32
    ).astype(jnp.bfloat16)
    row_log_weight_sum = (top + jnp.log(total))[..., 0]
    return (
        mixed.reshape(rows, kv_heads * group * HEAD_SIZE),
        row_log_weight_sum.transpose(1, 2, 0, 3).reshape(kv_heads * group, rows),
    )


def pool_branch(pool_rows, pool_tail, mixing, scales, group_start, first_pos):
    rows = pool_rows.shape[0]
    columns = pool_rows.shape[1]
    pool_reach = max(POOL_SPANS)
    extended = jnp.concatenate([pool_tail, pool_rows], 0).astype(jnp.float32)
    group_index = group_start + jnp.arange(columns) // POOL_CH
    span_table = jnp.array(POOL_SPANS, jnp.int32)
    matches = group_index[:, None] == jnp.arange(len(POOL_SPANS))[None, :]
    span_of_col = jnp.sum(jnp.where(matches, span_table[None, :], 0), axis=1)
    trailing = jnp.zeros((rows, columns), jnp.float32)
    for lag in range(pool_reach):
        trailing = trailing + jnp.where(
            lag < span_of_col[None, :], extended[pool_reach - lag : pool_reach - lag + rows], 0.0
        )
    position = first_pos + jnp.arange(rows)
    count = jnp.minimum(position[:, None] + 1, span_of_col[None, :]).astype(jnp.float32)
    centred = (trailing / count - extended[pool_reach:]).astype(jnp.bfloat16)
    grouped = centred.reshape(rows, columns // POOL_CH, POOL_CH)
    product = jnp.einsum(
        "rgc,gcd->rgd", grouped, mixing, preferred_element_type=jnp.float32
    ).reshape(rows, columns)
    return (product * scales).astype(jnp.bfloat16)


def local(
    tokens,
    norm_gain,
    query_weight,
    key_matrix,
    value_matrix,
    pool_in_weight,
    head_sink_logit,
    pool_mix,
    pool_gain,
    attn_out_weight,
    pool_out_weight,
):
    tp_index = lax.axis_index("tp")
    sp_index = lax.axis_index("sp")
    q_cols = query_weight.shape[1]
    kv_cols = key_matrix.shape[1]
    pool_cols = pool_in_weight.shape[1]
    q_heads = q_cols // HEAD_SIZE
    kv_heads = kv_cols // HEAD_SIZE
    groups_dev = pool_cols // POOL_CH
    full_query, full_key, full_value, full_pool = (
        lax.all_gather(query_weight, "sp", axis=0, tiled=True),
        lax.all_gather(key_matrix, "sp", axis=0, tiled=True),
        lax.all_gather(value_matrix, "sp", axis=0, tiled=True),
        lax.all_gather(pool_in_weight, "sp", axis=0, tiled=True),
    )
    values_f = lax.all_gather(tokens[0], "tp", axis=0, tiled=True).astype(jnp.float32)
    scale = lax.rsqrt(jnp.mean(values_f * values_f, axis=-1, keepdims=True) + EPSILON)
    normed = (values_f * scale * norm_gain).astype(jnp.bfloat16)
    outputs = [
        jnp.dot(normed, weight, preferred_element_type=jnp.float32).astype(jnp.bfloat16)
        for weight in (full_query, full_key, full_value, full_pool)
    ]
    projected = jnp.concatenate(outputs, axis=1)
    rows = projected.shape[0]
    first_pos = sp_index * rows
    query_rows = projected[:, :q_cols]
    key_rows = projected[:, q_cols : q_cols + kv_cols]
    value_rows = projected[:, q_cols + kv_cols : q_cols + 2 * kv_cols]
    pool_rows = projected[:, q_cols + 2 * kv_cols :]
    pool_reach = max(POOL_SPANS)
    sinks = lax.dynamic_slice_in_dim(head_sink_logit, tp_index * q_heads, q_heads, 0)
    mixing = lax.dynamic_slice_in_dim(pool_mix, tp_index * groups_dev, groups_dev, 0)
    scales = lax.dynamic_slice_in_dim(pool_gain, tp_index * pool_cols, pool_cols, 0)
    key_tail, value_tail, pool_tail = passed_along(
        (key_rows[rows - WINDOW :], value_rows[rows - WINDOW :], pool_rows[rows - pool_reach :]),
        "sp",
        1,
    )
    attn_part, log_part = windowed_attend(
        query_rows,
        key_rows,
        value_rows,
        key_tail,
        value_tail,
        sinks,
        kv_heads,
        q_heads // kv_heads,
        first_pos,
    )
    pool_part = pool_branch(pool_rows, pool_tail, mixing, scales, tp_index * groups_dev, first_pos)
    half_attn, half_pool = (
        lax.all_gather(attn_out_weight, "sp", axis=1, tiled=True),
        lax.all_gather(pool_out_weight, "sp", axis=1, tiled=True),
    )
    result = lax.psum_scatter(
        jnp.dot(attn_part, half_attn, preferred_element_type=jnp.float32)
        + jnp.dot(pool_part, half_pool, preferred_element_type=jnp.float32),
        "tp",
        scatter_dimension=0,
        tiled=True,
    ).astype(jnp.bfloat16)
    return (result[None], log_part[None])


def solution(mesh):
    in_specs = (
        P("fs", ("sp", "tp"), None),
        P(),
        P("sp", "tp"),
        P("sp", "tp"),
        P("sp", "tp"),
        P("sp", "tp"),
        P(),
        P(),
        P(),
        P("tp", "sp"),
        P("tp", "sp"),
    )
    out_specs = (P("fs", ("sp", "tp"), None), P("fs", "tp", "sp"))
    return jax.shard_map(local, mesh=mesh, in_specs=in_specs, out_specs=out_specs, check_vma=False)
```

profile of v0, /device:TPU:0, one launch (start us, length us, event | category | flops | bytes accessed | tf_op | source)
XLA Modules:
  0.0 243.1 jit_solution(15689682092924149541)
XLA Ops:
  10.8 17.6 %all_gather.23 = bf16[2048,128]{1,0:T(8,128)(2,1)S(1)} all-gather(bf16[512,128]{1,0:T(8,128)(2,1)} %param.15), channel_id=1, replica_groups=mesh['sp'=4,'fs'=4,'tp'=2] {'sp'}, dimensions={0}, use_global_device_ids=true | all-gather | bytes 655360 | tf_op jit(solution)/shard_map/all_gather | solution.py:115
  29.2 23.4 %all_gather.22 = bf16[2048,128]{1,0:T(8,128)(2,1)} all-gather(bf16[512,128]{1,0:T(8,128)(2,1)} %param.16), channel_id=1, replica_groups=mesh['sp'=4,'fs'=4,'tp'=2] {'sp'}, dimensions={0}, use_global_device_ids=true | all-gather | bytes 655360 | tf_op jit(solution)/shard_map/all_gather | solution.py:116
  53.9 2.2 fusion
  56.1 2.4 convolution_convert_fusion.2
  59.1 3.5 %collective-permute-start.1 = (bf16[128,128]{1,0:T(8,128)(2,1)}, bf16[128,128]{1,0:T(8,128)(2,1)}, u32[]{:S(2)}, u32[]{:S(2)}) collective-permute-start(bf16[128,128]{1,0:T(8,128)(2,1)} %slice.86), channel_id=1, source_target_pairs={{0,8},{8,16},{16,24},{1,9},{9,17},{17,25},{2,10},{10,18},{18,26},{... | collective-permute-start | bytes 98312 | tf_op jit(solution)/shard_map/ppermute | solution.py:16
  62.6 1.5 convolution_convert_fusion.3
  65.0 0.8 copy.45
  65.8 2.0 collective-permute-start
  71.3 5.5 %all-gather.7.cloned.1.call-done = bf16[2048,512]{1,0:T(8,128)(2,1)} async-done(((bf16[512,512]{1,0:T(8,128)(2,1)}), bf16[2048,512]{1,0:T(8,128)(2,1)}) %all-gather.7.cloned.1.call-update) | async-done | bytes 2097168 | tf_op jit(solution)/shard_map/all_gather | solution.py:114
  76.8 2.9 %convolution_convert_fusion.1 = bf16[512,512]{1,0:T(8,128)(2,1)S(1)} fusion(bf16[2048,512]{1,0:T(8,128)(2,1)} %all-gather.7.cloned.1.call-done, bf16[1,512,2048]{2,1,0:T(8,128)(2,1)S(1)} %copy-done.1, f32[2048]{0:T(1024)} %param.13, f32[512]{0:T(512)} %copy-done.23), kind=kOutput, calls=%fused_computation.13 | convolution fusion | flops 1078198272 | bytes 4728832 | tf_op jit(solution)/shard_map/dot_general | solution.py:123
  79.7 1.5 reshape.236
  81.3 2.3 fusion.4
  83.6 1.0 fusion.3
  84.7 1.2 fusion.7
  86.3 38.3 %all-gather.11.cloned.1.call-done = bf16[2048,512]{1,0:T(8,128)(2,1)} async-done(((bf16[512,512]{1,0:T(8,128)(2,1)}), bf16[2048,512]{1,0:T(8,128)(2,1)}) %all-gather.11.cloned.1.call-update) | async-done | bytes 2097168 | tf_op jit(solution)/shard_map/all_gather | solution.py:117
  124.6 2.9 %convolution_convert_fusion = bf16[512,512]{1,0:T(8,128)(2,1)S(1)} fusion(bf16[2048,512]{1,0:T(8,128)(2,1)} %all-gather.11.cloned.1.call-done, bf16[1,512,2048]{2,1,0:T(8,128)(2,1)S(1)} %copy-done.1, f32[2048]{0:T(1024)S(1)} %copy-done.28, f32[512]{0:T(512)S(1)} %copy-done.24), kind=kOutput, calls=%fused_computation.12 | convolution fusion | flops 1078198272 | bytes 4728832 | tf_op jit(solution)/shard_map/dot_general | solution.py:123
  128.3 2.4 collective-permute-start.2
  130.7 39.8 %all-gather.9.cloned.1.call-done = bf16[512,2048]{1,0:T(8,128)(2,1)} async-done(((bf16[512,512]{1,0:T(8,128)(2,1)}), bf16[512,2048]{1,0:T(8,128)(2,1)}) %all-gather.9.cloned.1.call-update) | async-done | bytes 2097168 | tf_op jit(solution)/shard_map/all_gather | solution.py:155
  170.6 4.9 %fusion.29 = f32[512,2048]{1,0:T(8,128)} fusion(bf16[512,2048]{1,0:T(8,128)(2,1)} %all-gather.9.cloned.1.call-done, bf16[64,8,4,128]{3,2,1,0:T(4,128)(2,1)S(1)} %bitcast.76), kind=kOutput, calls=%fused_computation.59 | convolution fusion | flops 1073741824 | bytes 6815744 | tf_op jit(solution)/shard_map/dot_general | solution.py:159
  175.8 3.0 %fusion.28 = bf16[512,512]{1,0:T(8,128)(2,1)S(1)} fusion(f32[528,512]{1,0:T(8,128)S(1)} %maximum_convert_fusion, s32[512]{0:T(512)S(1)} %select_reduce_fusion, s32[512]{0:T(512)S(1)} %add_add_fusion, pred[512]{0:T(512)(128)(4,1)S(1)} %copy-done.8, pred[512]{0:T(512)(128)(4,1)S(1)} %copy-done.9, pred[512]{0:T(512)(128)(4,1)S(1)} %copy-done.10, ...), kind=kLoop, calls=%fused_computation.55 | loop fusion | flops 9437184 | bytes 17313792 | tf_op jit(solution)/shard_map/convert_element_type | solution.py:84
  179.3 37.1 %all-gather.13.cloned.1.call-done = bf16[512,2048]{1,0:T(8,128)(2,1)} async-done(((bf16[512,512]{1,0:T(8,128)(2,1)}), bf16[512,2048]{1,0:T(8,128)(2,1)}) %all-gather.13.cloned.1.call-update) | async-done | bytes 2097168 | tf_op jit(solution)/shard_map/all_gather | solution.py:156
  216.4 6.1 %convolution_add_fusion = f32[512,2048]{1,0:T(8,128)} fusion(f32[512,2048]{1,0:T(8,128)} %fusion.29, bf16[512,512]{0,1:T(8,128)(2,1)S(1)} %fusion.25, bf16[512,2048]{1,0:T(8,128)(2,1)} %all-gather.13.cloned.1.call-done), kind=kOutput, calls=%fused_computation.9 | convolution fusion | flops 1074790400 | bytes 11010048 | tf_op jit(solution)/shard_map/dot_general | solution.py:160
  223.2 10.3 %reduce-scatter.2.cloned.1.call-done = f32[256,2048]{1,0:T(8,128)} async-done(((f32[512,2048]{1,0:T(8,128)}), f32[256,2048]{1,0:T(8,128)}) %reduce-scatter.2.cloned.1.call-update) | async-done | bytes 2097168 | tf_op jit(solution)/shard_map/reduce_scatter | solution.py:158
  233.5 2.7 %convert_bitcast_fusion = bf16[1,256,2048]{2,1,0:T(8,128)(2,1)} fusion(f32[256,2048]{1,0:T(8,128)} %reduce-scatter.2.cloned.1.call-done), kind=kLoop, calls=%fused_computation.54 | loop fusion | flops 524288 | bytes 3145728 | tf_op jit(solution)/shard_map/broadcast_in_dim | solution.py:165
  (106 shorter events, 13.3 us)
Async XLA Ops:
  7.2 171.7 %copy-start = (bf16[4,256,256]{2,1,0:T(8,128)(2,1)S(1)}, bf16[4,256,256]{2,1,0:T(8,128)(2,1)}, u32[]{:S(2)}) copy-start(bf16[4,256,256]{2,1,0:T(8,128)(2,1)} %param.19) | copy-start | bytes 1572868
  7.2 45.5 %copy-start.26 = (s32[4]{0:T(128)S(1)}, s32[4]{0:T(128)}, u32[]{:S(2)}) copy-start(s32[4]{0:T(128)} %constant.89.clone) | copy-start | bytes 52
  7.2 46.2 %copy-start.25 = (f32[1024]{0:T(1024)S(1)}, f32[1024]{0:T(1024)}, u32[]{:S(2)}) copy-start(f32[1024]{0:T(1024)} %param.20) | copy-start | bytes 12292
  7.2 48.9 %copy-start.27 = (f32[2048]{0:T(1024)S(1)}, f32[2048]{0:T(1024)}, u32[]{:S(2)}) copy-start(f32[2048]{0:T(1024)} %param.13) | copy-start | bytes 24580
  7.2 46.6 %all-gather.15.cloned.1.call-start = ((), (), s32[]{:S(2)}) async-start(), calls=%async_computation.6 | async-start | bytes 3145728 | tf_op jit(solution)/shard_map/all_gather | solution.py:119
  7.9 68.9 %all-gather.7.cloned.1.call-start = ((), (), s32[]{:S(2)}) async-start(), calls=%async_computation.1 | async-start | bytes 2621440 | tf_op jit(solution)/shard_map/all_gather | solution.py:114
  8.7 115.9 %all-gather.11.cloned.1.call-start = ((), (), s32[]{:S(2)}) async-start(), calls=%async_computation.3 | async-start | bytes 2621440 | tf_op jit(solution)/shard_map/all_gather | solution.py:117
  9.4 161.1 %all-gather.9.cloned.1.call-start = ((), (), s32[]{:S(2)}) async-start(), calls=%async_computation.2 | async-start | bytes 2621440 | tf_op jit(solution)/shard_map/all_gather | solution.py:155
  10.0 206.4 %all-gather.13.cloned.1.call-start = ((), (), s32[]{:S(2)}) async-start(), calls=%async_computation.4 | async-start | bytes 2621440 | tf_op jit(solution)/shard_map/all_gather | solution.py:156
  10.6 222.9 %reduce-scatter.2.cloned.1.call-start = ((), (), s32[]{:S(2)}) async-start(), calls=%async_computation.5 | async-start | bytes 6291456 | tf_op jit(solution)/shard_map/reduce_scatter | solution.py:158
  53.8 8.8 %copy-start.1 = (bf16[1,512,2048]{2,1,0:T(8,128)(2,1)S(1)}, bf16[1,512,2048]{2,1,0:T(8,128)(2,1)}, u32[]{:S(2)}) copy-start(bf16[1,512,2048]{2,1,0:T(8,128)(2,1)} %all-gather.15.cloned.1.call-done) | copy-start | bytes 6291460
  53.8 8.8 %copy-start.4 = (bf16[2048,128]{1,0:T(8,128)(2,1)S(1)}, bf16[2048,128]{1,0:T(8,128)(2,1)}, u32[]{:S(2)}) copy-start(bf16[2048,128]{1,0:T(8,128)(2,1)} %all_gather.22) | copy-start | bytes 1572868
  56.1 6.5 %copy-start.23 = (f32[512]{0:T(512)}, f32[512]{0:T(512)S(1)}, u32[]{:S(2)}) copy-start(f32[512]{0:T(512)S(1)} %add_rsqrt_fusion) | copy-start | bytes 6148
  59.1 9.4 %collective-permute-start.1 = (bf16[128,128]{1,0:T(8,128)(2,1)}, bf16[128,128]{1,0:T(8,128)(2,1)}, u32[]{:S(2)}, u32[]{:S(2)}) collective-permute-start(bf16[128,128]{1,0:T(8,128)(2,1)} %slice.86), channel_id=1, source_target_pairs={{0,8},{8,16},{16,24},{1,9},{9,17},{17,25},{2,10},{10,18},{18,26},{... | collective-permute-start | bytes 98312 | tf_op jit(solution)/shard_map/ppermute | solution.py:16
  65.8 4.6 %collective-permute-start = (bf16[128,128]{1,0:T(8,128)(2,1)}, bf16[128,128]{1,0:T(8,128)(2,1)S(1)}, u32[]{:S(2)}, u32[]{:S(2)}) collective-permute-start(bf16[128,128]{1,0:T(8,128)(2,1)} %slice.85), channel_id=1, source_target_pairs={{0,8},{8,16},{16,24},{1,9},{9,17},{17,25},{2,10},{10,18},{18,26},{... | collective-permute-start | bytes 98312 | tf_op jit(solution)/shard_map/ppermute | solution.py:16
  84.7 39.9 %copy-start.24 = (f32[512]{0:T(512)S(1)}, f32[512]{0:T(512)}, u32[]{:S(2)}) copy-start(f32[512]{0:T(512)} %copy-done.23) | copy-start | bytes 6148
  84.7 39.9 %copy-start.28 = (f32[2048]{0:T(1024)S(1)}, f32[2048]{0:T(1024)}, u32[]{:S(2)}) copy-start(f32[2048]{0:T(1024)} %param.13) | copy-start | bytes 24580
  128.3 47.2 %copy-start.3 = (bf16[512,512]{1,0:T(8,128)(2,1)S(1)}, bf16[512,512]{1,0:T(8,128)(2,1)}, u32[]{:S(2)}) copy-start(bf16[512,512]{1,0:T(8,128)(2,1)} %copy-done.2) | copy-start | bytes 1572868
  128.3 47.2 %collective-permute-start.2 = (bf16[16,512]{1,0:T(8,128)(2,1)S(1)}, bf16[16,512]{1,0:T(8,128)(2,1)S(1)}, u32[]{:S(2)}, u32[]{:S(2)}) collective-permute-start(bf16[16,512]{1,0:T(8,128)(2,1)S(1)} %slice.87), channel_id=1, source_target_pairs={{0,8},{8,16},{16,24},{1,9},{9,17},{17,25},{2,10},{10,18},{18,26},{... | collective-permute-start | bytes 49160 | tf_op jit(solution)/shard_map/ppermute | solution.py:16
  170.5 5.2 %copy-start.12 = (pred[512]{0:T(512)(128)(4,1)S(1)}, pred[512]{0:T(512)(128)(4,1)}, u32[]{:S(2)}) copy-start(pred[512]{0:T(512)(128)(4,1)} %get-tuple-element.7) | copy-start | bytes 1540
  170.5 5.2 %copy-start.13 = (pred[512]{0:T(512)(128)(4,1)S(1)}, pred[512]{0:T(512)(128)(4,1)}, u32[]{:S(2)}) copy-start(pred[512]{0:T(512)(128)(4,1)} %get-tuple-element.8) | copy-start | bytes 1540
  170.6 5.2 %copy-start.14 = (pred[512]{0:T(512)(128)(4,1)S(1)}, pred[512]{0:T(512)(128)(4,1)}, u32[]{:S(2)}) copy-start(pred[512]{0:T(512)(128)(4,1)} %get-tuple-element.9) | copy-start | bytes 1540
  170.6 5.2 %copy-start.15 = (pred[512]{0:T(512)(128)(4,1)S(1)}, pred[512]{0:T(512)(128)(4,1)}, u32[]{:S(2)}) copy-start(pred[512]{0:T(512)(128)(4,1)} %get-tuple-element.10) | copy-start | bytes 1540
  170.6 5.2 %copy-start.16 = (pred[512]{0:T(512)(128)(4,1)S(1)}, pred[512]{0:T(512)(128)(4,1)}, u32[]{:S(2)}) copy-start(pred[512]{0:T(512)(128)(4,1)} %get-tuple-element.11) | copy-start | bytes 1540
  (14 other events, 64.3 us)
Sparse Core Ops, SparseCore 0:
  9.6 13.2 all-gather.14
  24.5 52.2 all-gather.6
  78.4 46.1 all-gather.10
  126.0 44.4 all-gather.8
  171.9 44.4 all-gather.12
  222.7 10.8 reduce-scatter.1
where the time goes:
time: 244 us; the launch traced here: 243 us
  waiting for transfers between devices  134 us (55%)
  blocking collectives  41 us (17%)
  matrix products  24.4 us (10%)
  between operations  14.6 us (6%)
  other arithmetic  12.1 us (5%)
  local copies, waits for them, and re-layouts  8.64 us (4%)
  starting transfers between devices  8.09 us (3%)
    all_gather x1, waiting for transfers between devices, local(): lax.all_gather(attn_out_weight, 'sp', axis=1, tiled=True)  39.8 us
    all_gather x1, waiting for transfers between devices, local(): lax.all_gather(pool_in_weight, 'sp', axis=0, tiled=True)  38.3 us
    all_gather x1, waiting for transfers between devices, local(): lax.all_gather(pool_out_weight, 'sp', axis=1, tiled=True)  37.1 us
    all_gather x1, blocking collectives, local(): lax.all_gather(value_matrix, 'sp', axis=0, tiled=True)  23.4 us
    all_gather x1, blocking collectives, local(): lax.all_gather(key_matrix, 'sp', axis=0, tiled=True)  17.6 us
    reduce_scatter x1, waiting for transfers between devices, local(): lax.psum_scatter(jnp.dot(attn_part, half_attn, preferred_element_type=jnp...  10.3 us
    dot_general x4, matrix products, local(): jnp.dot(normed, weight, preferred_element_type=jnp.float32)  9.63 us
    ppermute x3, starting transfers between devices, passed_along(): return lax.ppermute(shard, axis, pairs)  7.87 us
  transfers between devices with their start and end apart: 9, of which 6 were waited for; matrix products, arithmetic and copies ran while one was open for 15% of the time, Pallas kernels for 0%

commit v1 on v0

--- a/solution.py
+++ b/solution.py
@@ -2,6 +2,7 @@
 import jax.numpy as jnp
 from jax import lax
 from jax.sharding import PartitionSpec as P
+from jax.lax import all_gather
 
 HEAD_SIZE = 64
 WINDOW = 128
@@ -152,7 +153,7 @@
     )
     pool_part = pool_branch(pool_rows, pool_tail, mixing, scales, tp_index * groups_dev, first_pos)
     half_attn, half_pool = (
-        lax.all_gather(attn_out_weight, "sp", axis=1, tiled=True),
+        jnp.concatenate(all_gather(attn_out_weight, "sp"), axis=1),
         lax.all_gather(pool_out_weight, "sp", axis=1, tiled=True),
     )
     result = lax.psum_scatter(

time: 244 us -> 244 us (level)
    all_gather x1, waiting for transfers between devices: 38.3 us -> 43.1 us  [local(): lax.all_gather(pool_in_weight, 'sp', axis=0, tiled=True)]
    all_gather x1, waiting for transfers between devices: 37.1 us -> 32.8 us  [local(): lax.all_gather(pool_out_weight, 'sp', axis=1, tiled=True)]
    reshape x0 -> x1, local copies, waits for them, and re-layouts: none -> 2.79 us  [local(): jnp.concatenate(all_gather(attn_out_weight, 'sp'), axis=1)]
where the time goes in v1:
time: 244 us; the launch traced here: 243 us
  waiting for transfers between devices  135 us (55%)
  blocking collectives  41 us (17%)
  matrix products  23.1 us (9%)
  between operations  14.7 us (6%)
  other arithmetic  12.1 us (5%)
  local copies, waits for them, and re-layouts  9.63 us (4%)
  starting transfers between devices  7.97 us (3%)
    all_gather x1, waiting for transfers between devices, local(): lax.all_gather(pool_in_weight, 'sp', axis=0, tiled=True)  43.1 us
    all_gather x1, waiting for transfers between devices, local(): all_gather(attn_out_weight, 'sp')  39.6 us
    all_gather x1, waiting for transfers between devices, local(): lax.all_gather(pool_out_weight, 'sp', axis=1, tiled=True)  32.8 us
    all_gather x1, blocking collectives, local(): lax.all_gather(value_matrix, 'sp', axis=0, tiled=True)  23.4 us
    all_gather x1, blocking collectives, local(): lax.all_gather(key_matrix, 'sp', axis=0, tiled=True)  17.6 us
    reduce_scatter x1, waiting for transfers between devices, local(): lax.psum_scatter(jnp.dot(attn_part, half_attn, preferred_element_type=jnp...  10.3 us
    dot_general x4, matrix products, local(): jnp.dot(normed, weight, preferred_element_type=jnp.float32)  10.3 us
    ppermute x3, starting transfers between devices, passed_along(): return lax.ppermute(shard, axis, pairs)  7.74 us
  transfers between devices with their start and end apart: 9, of which 6 were waited for; matrix products, arithmetic and copies ran while one was open for 15% of the time, Pallas kernels for 0%

profile of v1, /device:TPU:0, one launch (start us, length us, event | category | flops | bytes accessed | tf_op | source)
XLA Modules:
  0.0 243.1 jit_solution(13538314944485270732)
XLA Ops:
  10.8 17.6 %all_gather.26 = bf16[2048,128]{1,0:T(8,128)(2,1)S(1)} all-gather(bf16[512,128]{1,0:T(8,128)(2,1)} %param.15), channel_id=1, replica_groups=mesh['sp'=4,'fs'=4,'tp'=2] {'sp'}, dimensions={0}, use_global_device_ids=true | all-gather | bytes 655360 | tf_op jit(solution)/shard_map/all_gather | solution.py:116
  29.2 23.4 %all_gather.25 = bf16[2048,128]{1,0:T(8,128)(2,1)} all-gather(bf16[512,128]{1,0:T(8,128)(2,1)} %param.16), channel_id=1, replica_groups=mesh['sp'=4,'fs'=4,'tp'=2] {'sp'}, dimensions={0}, use_global_device_ids=true | all-gather | bytes 655360 | tf_op jit(solution)/shard_map/all_gather | solution.py:117
  53.9 2.2 fusion
  56.1 2.4 convolution_convert_fusion.2
  59.1 3.5 %collective-permute-start.1 = (bf16[128,128]{1,0:T(8,128)(2,1)}, bf16[128,128]{1,0:T(8,128)(2,1)}, u32[]{:S(2)}, u32[]{:S(2)}) collective-permute-start(bf16[128,128]{1,0:T(8,128)(2,1)} %slice.86), channel_id=1, source_target_pairs={{0,8},{8,16},{16,24},{1,9},{9,17},{17,25},{2,10},{10,18},{18,26},{... | collective-permute-start | bytes 98312 | tf_op jit(solution)/shard_map/ppermute | solution.py:17
  62.6 1.5 convolution_convert_fusion.3
  65.7 2.0 collective-permute-start
  67.7 0.8 copy.57
  71.2 5.6 %all-gather.8.cloned.1.call-done = bf16[2048,512]{1,0:T(8,128)(2,1)} async-done(((bf16[512,512]{1,0:T(8,128)(2,1)}), bf16[2048,512]{1,0:T(8,128)(2,1)}) %all-gather.8.cloned.1.call-update) | async-done | bytes 2097168 | tf_op jit(solution)/shard_map/all_gather | solution.py:115
  76.8 2.9 %convolution_convert_fusion.1 = bf16[512,512]{1,0:T(8,128)(2,1)S(1)} fusion(bf16[2048,512]{1,0:T(8,128)(2,1)} %all-gather.8.cloned.1.call-done, bf16[1,512,2048]{2,1,0:T(8,128)(2,1)S(1)} %copy-done.1, f32[2048]{0:T(1024)} %param.13, f32[512]{0:T(512)} %copy-done.21), kind=kOutput, calls=%fused_computation.13 | convolution fusion | flops 1078198272 | bytes 4728832 | tf_op jit(solution)/shard_map/dot_general | solution.py:124
  80.3 1.9 fusion.4
  82.3 1.0 fusion.3
  83.4 1.2 fusion.7
  85.0 39.6 %all-gather.16.cloned.1.call-done = bf16[2048,512]{1,0:T(8,128)(2,1)} async-done(((bf16[512,512]{1,0:T(8,128)(2,1)}), bf16[2048,512]{1,0:T(8,128)(2,1)}) %all-gather.16.cloned.1.call-update) | async-done | bytes 2097168 | tf_op jit(solution)/shard_map/all_gather | solution.py:156
  124.6 2.8 %copy.66 = bf16[512,4,512]{0,2,1:T(8,128)(2,1)S(1)} copy(bf16[512,4,512]{2,0,1:T(8,128)(2,1)} %bitcast.81) | data formatting | bytes 4194304 | tf_op jit(solution)/shard_map/reshape | solution.py:156
  127.4 43.1 %all-gather.10.cloned.1.call-done = bf16[2048,512]{1,0:T(8,128)(2,1)} async-done(((bf16[512,512]{1,0:T(8,128)(2,1)}), bf16[2048,512]{1,0:T(8,128)(2,1)}) %all-gather.10.cloned.1.call-update) | async-done | bytes 2097168 | tf_op jit(solution)/shard_map/all_gather | solution.py:118
  170.5 3.5 %convolution_convert_fusion = bf16[512,512]{1,0:T(8,128)(2,1)S(1)} fusion(bf16[2048,512]{1,0:T(8,128)(2,1)} %all-gather.10.cloned.1.call-done, bf16[1,512,2048]{2,1,0:T(8,128)(2,1)} %all-gather.14.cloned.1.call-done, f32[2048]{0:T(1024)S(1)} %copy-done.26, f32[512]{0:T(512)S(1)} %copy-done.22), kind=kOutput, calls=%fused_computation.12 | convolution fusion | flops 1078198272 | bytes 4728832 | tf_op jit(solution)/shard_map/dot_general | solution.py:124
  174.1 2.3 collective-permute-start.2
  176.5 3.3 %fusion.29 = f32[512,2048]{1,0:T(8,128)} fusion(bf16[512,2048]{0,1:T(8,128)(2,1)S(1)} %bitcast.79, bf16[64,8,4,128]{3,2,1,0:T(4,128)(2,1)S(1)} %bitcast.80), kind=kOutput, calls=%fused_computation.59 | convolution fusion | flops 1073741824 | bytes 6815744 | tf_op jit(solution)/shard_map/dot_general | solution.py:160
  180.1 3.0 %fusion.28 = bf16[512,512]{1,0:T(8,128)(2,1)S(1)} fusion(f32[528,512]{1,0:T(8,128)S(1)} %maximum_convert_fusion, s32[512]{0:T(512)S(1)} %select_reduce_fusion, s32[512]{0:T(512)S(1)} %add_add_fusion, pred[512]{0:T(512)(128)(4,1)S(1)} %copy-done.6, pred[512]{0:T(512)(128)(4,1)S(1)} %copy-done.7, pred[512]{0:T(512)(128)(4,1)S(1)} %copy-done.8, ...), kind=kLoop, calls=%fused_computation.55 | loop fusion | flops 9437184 | bytes 17313792 | tf_op jit(solution)/shard_map/convert_element_type | solution.py:85
  183.6 32.8 %all-gather.12.cloned.1.call-done = bf16[512,2048]{1,0:T(8,128)(2,1)} async-done(((bf16[512,512]{1,0:T(8,128)(2,1)}), bf16[512,2048]{1,0:T(8,128)(2,1)}) %all-gather.12.cloned.1.call-update) | async-done | bytes 2097168 | tf_op jit(solution)/shard_map/all_gather | solution.py:157
  216.4 6.1 %convolution_add_fusion = f32[512,2048]{1,0:T(8,128)} fusion(f32[512,2048]{1,0:T(8,128)} %fusion.29, bf16[512,512]{0,1:T(8,128)(2,1)S(1)} %fusion.25, bf16[512,2048]{1,0:T(8,128)(2,1)} %all-gather.12.cloned.1.call-done), kind=kOutput, calls=%fused_computation.9 | convolution fusion | flops 1074790400 | bytes 11010048 | tf_op jit(solution)/shard_map/dot_general | solution.py:161
  223.2 10.3 %reduce-scatter.2.cloned.1.call-done = f32[256,2048]{1,0:T(8,128)} async-done(((f32[512,2048]{1,0:T(8,128)}), f32[256,2048]{1,0:T(8,128)}) %reduce-scatter.2.cloned.1.call-update) | async-done | bytes 2097168 | tf_op jit(solution)/shard_map/reduce_scatter | solution.py:159
  233.5 2.7 %convert_bitcast_fusion = bf16[1,256,2048]{2,1,0:T(8,128)(2,1)} fusion(f32[256,2048]{1,0:T(8,128)} %reduce-scatter.2.cloned.1.call-done), kind=kLoop, calls=%fused_computation.54 | loop fusion | flops 524288 | bytes 3145728 | tf_op jit(solution)/shard_map/broadcast_in_dim | solution.py:166
  (103 shorter events, 13.0 us)
Async XLA Ops:
  7.2 175.9 %copy-start = (bf16[4,256,256]{2,1,0:T(8,128)(2,1)S(1)}, bf16[4,256,256]{2,1,0:T(8,128)(2,1)}, u32[]{:S(2)}) copy-start(bf16[4,256,256]{2,1,0:T(8,128)(2,1)} %param.19) | copy-start | bytes 1572868
  7.2 45.5 %copy-start.24 = (s32[4]{0:T(128)S(1)}, s32[4]{0:T(128)}, u32[]{:S(2)}) copy-start(s32[4]{0:T(128)} %constant.89.clone) | copy-start | bytes 52
  7.2 46.2 %copy-start.23 = (f32[1024]{0:T(1024)S(1)}, f32[1024]{0:T(1024)}, u32[]{:S(2)}) copy-start(f32[1024]{0:T(1024)} %param.20) | copy-start | bytes 12292
  7.2 48.9 %copy-start.25 = (f32[2048]{0:T(1024)S(1)}, f32[2048]{0:T(1024)}, u32[]{:S(2)}) copy-start(f32[2048]{0:T(1024)} %param.13) | copy-start | bytes 24580
  7.2 46.6 %all-gather.14.cloned.1.call-start = ((), (), s32[]{:S(2)}) async-start(), calls=%async_computation.5 | async-start | bytes 3145728 | tf_op jit(solution)/shard_map/all_gather | solution.py:120
  7.9 68.9 %all-gather.8.cloned.1.call-start = ((), (), s32[]{:S(2)}) async-start(), calls=%async_computation.1 | async-start | bytes 2621440 | tf_op jit(solution)/shard_map/all_gather | solution.py:115
  8.7 115.9 %all-gather.16.cloned.1.call-start = ((), (), s32[]{:S(2)}) async-start(), calls=%async_computation.6 | async-start | bytes 2621440 | tf_op jit(solution)/shard_map/all_gather | solution.py:156
  9.4 161.1 %all-gather.10.cloned.1.call-start = ((), (), s32[]{:S(2)}) async-start(), calls=%async_computation.2 | async-start | bytes 2621440 | tf_op jit(solution)/shard_map/all_gather | solution.py:118
  10.0 206.4 %all-gather.12.cloned.1.call-start = ((), (), s32[]{:S(2)}) async-start(), calls=%async_computation.3 | async-start | bytes 2621440 | tf_op jit(solution)/shard_map/all_gather | solution.py:157
  10.6 222.9 %reduce-scatter.2.cloned.1.call-start = ((), (), s32[]{:S(2)}) async-start(), calls=%async_computation.4 | async-start | bytes 6291456 | tf_op jit(solution)/shard_map/reduce_scatter | solution.py:159
  53.8 8.8 %copy-start.1 = (bf16[1,512,2048]{2,1,0:T(8,128)(2,1)S(1)}, bf16[1,512,2048]{2,1,0:T(8,128)(2,1)}, u32[]{:S(2)}) copy-start(bf16[1,512,2048]{2,1,0:T(8,128)(2,1)} %all-gather.14.cloned.1.call-done) | copy-start | bytes 6291460
  53.8 8.8 %copy-start.2 = (bf16[2048,128]{1,0:T(8,128)(2,1)S(1)}, bf16[2048,128]{1,0:T(8,128)(2,1)}, u32[]{:S(2)}) copy-start(bf16[2048,128]{1,0:T(8,128)(2,1)} %all_gather.25) | copy-start | bytes 1572868
  56.1 6.5 %copy-start.21 = (f32[512]{0:T(512)}, f32[512]{0:T(512)S(1)}, u32[]{:S(2)}) copy-start(f32[512]{0:T(512)S(1)} %add_rsqrt_fusion) | copy-start | bytes 6148
  59.1 9.5 %collective-permute-start.1 = (bf16[128,128]{1,0:T(8,128)(2,1)}, bf16[128,128]{1,0:T(8,128)(2,1)}, u32[]{:S(2)}, u32[]{:S(2)}) collective-permute-start(bf16[128,128]{1,0:T(8,128)(2,1)} %slice.86), channel_id=1, source_target_pairs={{0,8},{8,16},{16,24},{1,9},{9,17},{17,25},{2,10},{10,18},{18,26},{... | collective-permute-start | bytes 98312 | tf_op jit(solution)/shard_map/ppermute | solution.py:17
  65.7 4.6 %collective-permute-start = (bf16[128,128]{1,0:T(8,128)(2,1)}, bf16[128,128]{1,0:T(8,128)(2,1)S(1)}, u32[]{:S(2)}, u32[]{:S(2)}) collective-permute-start(bf16[128,128]{1,0:T(8,128)(2,1)} %slice.85), channel_id=1, source_target_pairs={{0,8},{8,16},{16,24},{1,9},{9,17},{17,25},{2,10},{10,18},{18,26},{... | collective-permute-start | bytes 98312 | tf_op jit(solution)/shard_map/ppermute | solution.py:17
  84.6 86.0 %copy-start.22 = (f32[512]{0:T(512)S(1)}, f32[512]{0:T(512)}, u32[]{:S(2)}) copy-start(f32[512]{0:T(512)} %copy-done.21) | copy-start | bytes 6148
  84.6 86.0 %copy-start.26 = (f32[2048]{0:T(1024)S(1)}, f32[2048]{0:T(1024)}, u32[]{:S(2)}) copy-start(f32[2048]{0:T(1024)} %param.13) | copy-start | bytes 24580
  174.1 5.7 %collective-permute-start.2 = (bf16[16,512]{1,0:T(8,128)(2,1)S(1)}, bf16[16,512]{1,0:T(8,128)(2,1)S(1)}, u32[]{:S(2)}, u32[]{:S(2)}) collective-permute-start(bf16[16,512]{1,0:T(8,128)(2,1)S(1)} %slice.87), channel_id=1, source_target_pairs={{0,8},{8,16},{16,24},{1,9},{9,17},{17,25},{2,10},{10,18},{18,26},{... | collective-permute-start | bytes 49160 | tf_op jit(solution)/shard_map/ppermute | solution.py:17
  176.3 3.6 %copy-start.5 = (pred[512]{0:T(512)(128)(4,1)S(1)}, pred[512]{0:T(512)(128)(4,1)}, u32[]{:S(2)}) copy-start(pred[512]{0:T(512)(128)(4,1)} %get-tuple-element.2) | copy-start | bytes 1540
  176.3 3.6 %copy-start.6 = (pred[512]{0:T(512)(128)(4,1)S(1)}, pred[512]{0:T(512)(128)(4,1)}, u32[]{:S(2)}) copy-start(pred[512]{0:T(512)(128)(4,1)} %get-tuple-element.3) | copy-start | bytes 1540
  176.4 3.6 %copy-start.7 = (pred[512]{0:T(512)(128)(4,1)S(1)}, pred[512]{0:T(512)(128)(4,1)}, u32[]{:S(2)}) copy-start(pred[512]{0:T(512)(128)(4,1)} %get-tuple-element.4) | copy-start | bytes 1540
  176.4 3.6 %copy-start.8 = (pred[512]{0:T(512)(128)(4,1)S(1)}, pred[512]{0:T(512)(128)(4,1)}, u32[]{:S(2)}) copy-start(pred[512]{0:T(512)(128)(4,1)} %get-tuple-element.5) | copy-start | bytes 1540
  176.4 3.6 %copy-start.9 = (pred[512]{0:T(512)(128)(4,1)S(1)}, pred[512]{0:T(512)(128)(4,1)}, u32[]{:S(2)}) copy-start(pred[512]{0:T(512)(128)(4,1)} %get-tuple-element.6) | copy-start | bytes 1540
  176.4 3.6 %copy-start.10 = (pred[512]{0:T(512)(128)(4,1)S(1)}, pred[512]{0:T(512)(128)(4,1)}, u32[]{:S(2)}) copy-start(pred[512]{0:T(512)(128)(4,1)} %get-tuple-element.7) | copy-start | bytes 1540
  (12 other events, 42.0 us)
Sparse Core Ops, SparseCore 0:
  9.6 13.2 all-gather.13
  24.5 52.2 all-gather.7
  78.4 46.1 all-gather.15
  126.0 44.4 all-gather.9
  171.9 44.4 all-gather.11
  222.7 10.8 reduce-scatter.1
